TPU v7x, 32 devices: a whole 2x2x4 slice. The times are simulated.
32 devices in a mesh: fs: 4 (over z), rep: 4 (over y, x), tp: 2 (over core).
Axes of the slice: x: 2, y: 2, z: 4, core: 2. Of those that a mesh axis runs over, the one named last changes fastest.
Arguments:
- query_input: bfloat16 [16384, 4096], P(('fs', 'rep')), may hold values from -6 to 6
- query_cotangent: bfloat16 [16384, 1024], P(('fs', 'rep'), 'tp'), may hold values from -0.046875 to 0.046875
- branch_output: bfloat16 [16384, 2048], P(('fs', 'rep')), may hold values from -6 to 6
- layer_cotangent: bfloat16 [16384, 4096], P(('fs', 'rep'), 'tp'), may hold values from -0.046875 to 0.046875
- query_weight: float32 [4096, 1024], P(('rep', 'fs'), 'tp'), may hold values from -0.09375 to 0.09375
- output_weight: float32 [2048, 4096], P(('rep', 'fs'), 'tp'), may hold values from -0.125 to 0.125
- query_basis: bfloat16 [4096, 512], P(('rep', 'fs')), may hold values from -0.09375 to 0.09375
- output_basis: bfloat16 [2048, 512], P(('rep', 'fs')), may hold values from -0.125 to 0.125
- query_first: float32 [512, 1024], P(('rep', 'fs'), 'tp'), may hold values from -20 to 20
- query_second: float32 [512, 1024], P(('rep', 'fs'), 'tp'), may hold values from 0.25 to 2
- output_first: float32 [512, 4096], P(('rep', 'fs'), 'tp'), may hold values from -20 to 20
- output_second: float32 [512, 4096], P(('rep', 'fs'), 'tp'), may hold values from 0.25 to 2
Outputs:
- query_update: float32 [4096, 1024], P(('rep', 'fs'), 'tp')
- output_update: float32 [2048, 4096], P(('rep', 'fs'), 'tp')
- query_first_next: float32 [512, 1024], P(('rep', 'fs'), 'tp')
- query_second_next: float32 [512, 1024], P(('rep', 'fs'), 'tp')
- output_first_next: float32 [512, 4096], P(('rep', 'fs'), 'tp')
- output_second_next: float32 [512, 4096], P(('rep', 'fs'), 'tp')
- query_copy: bfloat16 [4096, 1024], P('rep', 'tp')
- output_copy: bfloat16 [2048, 4096], P('rep', 'tp')
All inputs are finite; a program needn't handle non-finite values.
Results may differ from a plain program's by a relative error of at most 0.0055.
Values may be sent and summed in bfloat16 or wider, within the bound.
No kernel may reach another device: no remote copies, remote signals or barrier semaphores. Data moves between devices by JAX's collectives and lax.ppermute only.
A program may use at most 128 MiB of HBM per device.

v0:
```python
import functools

import jax
import jax.numpy as jnp
from jax import lax
from jax.experimental import pallas as pl
from jax.experimental.pallas import tpu as pltpu
from jax.sharding import PartitionSpec as P


beta_first = 0.6
beta_second = 0.8
step_rate = 0.01
small_eps = 1e-06

f32 = jnp.float32
bf16 = jnp.bfloat16


def dot_rows(left, right):
    return lax.dot_general(left, right, (((0,), (0,)), ((), ())), preferred_element_type=f32)


def after(value, *others):
    return lax.optimization_barrier((value, *others))[0]


def finish_kernel(nf, nr, fold, rows, place_ref, scale_ref, basis_ref, *refs):
    pieces, weights = refs[: nr + 1], refs[nr + 1 : nr + 1 + nf]
    update_ref, copy_ref, spread_ref, product_ref = refs[nr + 1 + nf :]
    step, steps = pl.program_id(0), pl.num_programs(0)
    depth = pieces[0].shape[0]
    for k in range(nr - 1):
        spread_ref[k * depth : (k + 1) * depth, :] = pieces[k][...]

    @pl.when(step < steps // 2)
    def _():
        spread_ref[(nr - 1) * depth :, :] = pieces[nr - 1][...]

    @pl.when(step >= steps // 2)
    def _():
        spread_ref[(nr - 1) * depth :, :] = pieces[nr][...]

    product = jnp.dot(basis_ref[...], spread_ref[...], preferred_element_type=f32)
    product_ref[...] = scale_ref[0, 0] * product
    part = rows // fold
    for s in range(nf):
        source = lax.rem(place_ref[0] + (nf - s), nf)
        for n in range(fold):
            here = pl.ds(pl.multiple_of(source * rows + n * part, part), part)
            update = product_ref[here, :]
            weight = weights[s][:, n, :] if fold > 1 else weights[s][...]
            copy_ref[here, :] = (weight.astype(f32) - step_rate * update).astype(bf16)
    mine = pl.ds(pl.multiple_of(place_ref[0] * rows, rows), rows)
    update_ref[...] = product_ref[mine, :]


def finish(nf, nr, place, scale, basis, pieces, weights):
    depth, columns = pieces[0].shape
    rows = weights[0].shape[0]
    steps = 4 if columns % (4 * 256) == 0 else 2
    width = columns // steps
    half = steps // 2
    column = lambda s, p: (0, s)
    whole = lambda s, p: (0, 0)
    in_specs = [
        pl.BlockSpec((1, 1), whole, memory_space=pltpu.SMEM),
        pl.BlockSpec(basis.shape, whole),
        *[pl.BlockSpec((depth, width), column) for _ in range(nr - 1)],
        pl.BlockSpec((depth, width), lambda s, p: (0, jnp.minimum(s, half - 1))),
        pl.BlockSpec((depth, width), lambda s, p: (0, jnp.maximum(s - half, 0))),
        *[pl.BlockSpec((rows, width), column) for _ in weights],
    ]
    return pl.pallas_call(
        functools.partial(finish_kernel, nf, nr, 1, rows),
        grid_spec=pltpu.PrefetchScalarGridSpec(
            num_scalar_prefetch=1,
            grid=(steps,),
            in_specs=in_specs,
            out_specs=[
                pl.BlockSpec((rows, width), column),
                pl.BlockSpec((nf * rows, width), column),
            ],
            scratch_shapes=[
                pltpu.VMEM((nr * depth, width), bf16),
                pltpu.VMEM((nf * rows, width), f32),
            ],
        ),
        out_shape=[
            jax.ShapeDtypeStruct((rows, columns), f32),
            jax.ShapeDtypeStruct((nf * rows, columns), bf16),
        ],
    )(place.reshape(1), scale, basis, *pieces, *weights)


def make_body(nf, nr, nt):
    assert nr == 4 and nt == 2

    def flip(value, bits):
        return lax.ppermute(value, "rep", [(k, k ^ bits) for k in range(nr)])

    def swap(value):
        return lax.ppermute(value, "tp", [(0, 1), (1, 0)])

    def shift(value, step):
        return lax.ppermute(value, "fs", [(k, (k + step) % nf) for k in range(nf)])

    def body(
        query_input,
        query_cotangent,
        branch_output,
        layer_cotangent,
        query_weight,
        output_weight,
        query_basis,
        output_basis,
        query_first,
        query_second,
        output_first,
        output_second,
    ):
        place = lax.axis_index("fs")
        rep = lax.axis_index("rep")
        core = lax.axis_index("tp")
        low, high = rep % 2, rep // 2
        mine = high == core

        def natural(blocks):
            rows, columns = blocks[0].shape
            at = lax.broadcasted_iota(jnp.int32, (nf, 1, 1), 0)
            whole = jnp.broadcast_to(blocks[-1][None], (nf, rows, columns))
            for s in range(nf - 1):
                whole = jnp.where(at == (place + nf - s) % nf, blocks[s][None], whole)
            return whole.reshape(nf * rows, columns)

        def by_rep(blocks):
            rows, columns = blocks[0].shape
            whole = jnp.zeros((nr * rows, columns), blocks[0].dtype)
            for bits, value in enumerate(blocks):
                whole = lax.dynamic_update_slice(whole, value, ((rep ^ bits) * rows, 0))
            return whole

        def relative(own, other):
            kept, sent = jnp.where(mine, own, other), jnp.where(mine, other, own)
            quarter = kept.shape[1] // 2
            rows = kept.shape[0]

            def part(value, bit):
                return lax.dynamic_slice(value, (0, bit * quarter), (rows, quarter))

            return [part(kept, low), part(kept, 1 - low), part(sent, low), part(sent, 1 - low)]

        def half_basis(basis):
            half = basis.shape[1] // nt
            return lax.dynamic_slice(basis, (0, core * half), (basis.shape[0], half))

        def along_fs(value):
            return [value] + [shift(value, s) for s in range(1, nf)]

        def project(inner, other, cotangent):
            here, by_x, by_y, far = relative(inner, other)
            half = cotangent.shape[1] // 2
            left, right = cotangent[:, :half], cotangent[:, half:]
            block = here.shape[1]
            both = lambda a, b: jnp.concatenate([a, b], axis=1)
            got = flip(dot_rows(both(by_x, far), left).astype(bf16), 1)
            got_other = flip(dot_rows(both(by_y, far), right).astype(bf16), 2)
            first = dot_rows(both(here, by_y), left) + got.astype(f32)
            second = dot_rows(both(here, by_x), right) + got_other.astype(f32)
            first_more = flip(first[block:].astype(bf16), 2).astype(f32)
            second_more = flip(second[block:].astype(bf16), 1).astype(f32)
            first, second = first[:block] + first_more, second[:block] + second_more
            total = jnp.concatenate([first, second], axis=1)
            rows = block // nf

            def rows_of(step):
                at = (place + step) % nf * rows
                return lax.dynamic_slice(total, (at, 0), (rows, total.shape[1]))

            arrived = [shift(rows_of(s).astype(bf16), s) for s in range(1, nf)]
            projected = rows_of(0)
            for value in arrived:
                projected = projected + value.astype(f32)
            return projected

        def moments(first, second, projected):
            first_next = beta_first * first + (1.0 - beta_first) * projected
            second_next = beta_second * second + (1.0 - beta_second) * projected * projected
            rounded = (first_next / jnp.sqrt(second_next)).astype(bf16)
            return first_next, second_next, rounded

        def squares(block):
            wide = block.astype(f32)
            return jnp.sum(wide * wide).reshape(1, 1)

        basis_o = natural(along_fs(half_basis(output_basis)))
        basis_q = natural(along_fs(half_basis(query_basis)))
        others_o = [flip(basis_o, 1), flip(basis_o, 2), flip(basis_o, 3)]
        x_q, y_q = flip(basis_q, 1), flip(basis_q, 2)
        split = basis_q.shape[0] // 2
        far_q = [flip(y_q[:split], 1), flip(x_q[split:], 2)]
        whole_o = by_rep([basis_o, *others_o])
        whole_q = by_rep([basis_q, x_q, y_q, jnp.concatenate(far_q, axis=0)])

        fold = query_weight.shape[0] // output_weight.shape[0]
        rows_o, columns_o = output_weight.shape
        columns_q = query_weight.shape[1]
        packed = [output_weight] + [
            query_weight[n * rows_o : (n + 1) * rows_o] for n in range(fold)
        ]
        ring = [after(jnp.concatenate(packed, axis=1).astype(bf16), basis_q)]

        def turn():
            ring.append(shift(ring[-1], 1))

        inner_o = jnp.dot(branch_output, whole_o, preferred_element_type=f32).astype(bf16)
        other_o = swap(inner_o)
        projected_o = project(inner_o, other_o, layer_cotangent)
        inner_q = jnp.dot(query_input, whole_q, preferred_element_type=f32).astype(bf16)
        other_q = swap(inner_q)
        projected_q = project(inner_q, other_q, query_cotangent)
        late_o, late_q = lax.optimization_barrier((basis_o, basis_q, inner_q))[:2]
        order_o = jnp.concatenate(relative(late_o, swap(late_o)), axis=1)
        order_q = jnp.concatenate(relative(late_q, swap(late_q)), axis=1)

        first_o, second_o, rounded_o = moments(output_first, output_second, projected_o)
        first_q, second_q, rounded_q = moments(query_first, query_second, projected_q)
        block_o = natural(along_fs(rounded_o))
        block_q = natural(along_fs(rounded_q))

        for n in range(1, nf):
            if n == nf - 1:
                ring[-1] = after(ring[-1], block_o)
            turn()

        total = jnp.concatenate([squares(block_q), squares(block_o)], axis=1)
        total = total + swap(total)
        total = total + flip(total, 1)
        total = total + flip(total, 2)

        def spread(block, x, y):
            cut = block.shape[1] // 2
            return [block, x, y, flip(y[:, :cut], 1), flip(x[:, cut:], 2)]

        x_o, y_o = flip(block_o, 1), flip(block_o, 2)
        x_q, y_q = flip(block_q, 1), flip(block_q, 2)
        spread_o = spread(block_o, x_o, y_o)
        spread_q = spread(block_q, x_q, y_q)
        weights_o = [value[:, :columns_o] for value in ring]
        weights_q = [
            jnp.concatenate(
                [
                    value[:, columns_o + n * columns_q : columns_o + (n + 1) * columns_q]
                    for n in range(fold)
                ],
                axis=0,
            )
            for value in ring
        ]

        def end(total, order, pieces, weights):
            depth, columns = pieces[0].shape[0] * nr, pieces[0].shape[1]
            scale = lax.rsqrt(total / (depth * columns * nt) + small_eps)
            return finish(nf, nr, place, scale, order, pieces, weights)

        update_q, copy_q = end(total[:, :1], order_q, spread_q, weights_q)
        update_o, copy_o = end(total[:, 1:], order_o, spread_o, weights_o)
        return (update_q, update_o, first_q, second_q, first_o, second_o, copy_q, copy_o)

    return body


def solution(mesh):
    tokens, columns = P(("fs", "rep"), None), P(("fs", "rep"), "tp")
    rows, both = P(("rep", "fs"), None), P(("rep", "fs"), "tp")
    in_specs = (tokens, columns, tokens, columns, both, both, rows, rows, both, both, both, both)
    out_specs = (both,) * 6 + (P("rep", "tp"),) * 2
    nf = mesh.shape["fs"]
    body = make_body(nf, mesh.shape["rep"], mesh.shape["tp"])

    return jax.shard_map(body, mesh=mesh, in_specs=in_specs, out_specs=out_specs, check_vma=False)
```

profile of v0, /device:TPU:0, one launch (start us, length us, event | category | flops | bytes accessed | tf_op | source)
XLA Modules:
  0.0 196.9 jit_solution(17600127134932695946)
XLA Ops:
  1.7 5.1 %collective-permute-start.20 = (bf16[128,256]{1,0:T(8,128)(2,1)S(1)}, bf16[128,256]{1,0:T(8,128)(2,1)S(1)}, u32[]{:S(2)}, u32[]{:S(2)}) collective-permute-start(bf16[128,256]{1,0:T(8,128)(2,1)S(1)} %constant_dynamic-slice_fusion.12), channel_id=1, source_target_pairs={{0,24},{8,0},{16,8},{24,16},{1,25},{9,1},{17,9},{25,17},{2,26},{10... | collective-permute-start | bytes 196616 | tf_op jit(solution)/shard_map/ppermute | solution.py:106
  7.8 2.9 %collective-permute-start.2 = (bf16[256,256]{1,0:T(8,128)(2,1)S(1)}, bf16[256,256]{1,0:T(8,128)(2,1)S(1)}, u32[]{:S(2)}, u32[]{:S(2)}) collective-permute-start(bf16[256,256]{1,0:T(8,128)(2,1)S(1)} %constant_dynamic-slice_fusion.17), channel_id=1, source_target_pairs={{0,24},{8,0},{16,8},{24,16},{1,25},{9,1},{17,9},{25,17},{2,26},{10... | collective-permute-start | bytes 393224 | tf_op jit(solution)/shard_map/ppermute | solution.py:106
  10.8 2.7 %collective-permute-done.19 = bf16[128,256]{1,0:T(8,128)(2,1)S(1)} collective-permute-done((bf16[128,256]{1,0:T(8,128)(2,1)S(1)}, bf16[128,256]{1,0:T(8,128)(2,1)S(1)}, u32[]{:S(2)}, u32[]{:S(2)}) %collective-permute-start.19) | collective-permute-done | bytes 65568 | tf_op jit(solution)/shard_map/ppermute | solution.py:106
  16.6 1.9 collective-permute-start.1
  18.5 3.4 %collective-permute-start = (bf16[256,256]{1,0:T(8,128)(2,1)S(1)}, bf16[256,256]{1,0:T(8,128)(2,1)S(1)}, u32[]{:S(2)}, u32[]{:S(2)}) collective-permute-start(bf16[256,256]{1,0:T(8,128)(2,1)S(1)} %constant_dynamic-slice_fusion.17), channel_id=1, source_target_pairs={{0,16},{8,24},{16,0},{24,8},{1,17},{9,25},{17,1},{25,9},{2,18},{10... | collective-permute-start | bytes 393224 | tf_op jit(solution)/shard_map/ppermute | solution.py:106
  24.9 2.2 %collective-permute-done = bf16[256,256]{1,0:T(8,128)(2,1)S(1)} collective-permute-done((bf16[256,256]{1,0:T(8,128)(2,1)S(1)}, bf16[256,256]{1,0:T(8,128)(2,1)S(1)}, u32[]{:S(2)}, u32[]{:S(2)}) %collective-permute-start) | collective-permute-done | bytes 131104 | tf_op jit(solution)/shard_map/ppermute | solution.py:106
  31.4 2.7 %collective-permute-done.22 = bf16[512,256]{1,0:T(8,128)(2,1)} collective-permute-done((bf16[512,256]{1,0:T(8,128)(2,1)S(1)}, bf16[512,256]{1,0:T(8,128)(2,1)}, u32[]{:S(2)}, u32[]{:S(2)}) %collective-permute-start.22) | collective-permute-done | bytes 262176 | tf_op jit(solution)/shard_map/ppermute | solution.py:100
  37.4 3.3 %fusion.21 = bf16[1024,256]{1,0:T(8,128)(2,1)} fusion(bf16[1024,2048]{1,0:T(8,128)(2,1)S(1)} %copy-done.23, bf16[2048,256]{1,0:T(8,128)(2,1)} %constant_dynamic-update-slice_fusion), kind=kOutput, calls=%fused_computation.23 | convolution fusion | flops 1074003968 | bytes 5767168 | tf_op jit(solution)/shard_map/dot_general | solution.py:216
  53.2 2.3 %fusion.20 = bf16[1024,256]{1,0:T(8,128)(2,1)S(1)} fusion(bf16[1024,4096]{1,0:T(8,128)(2,1)S(1)} %copy-done.22, bf16[4096,256]{1,0:T(8,128)(2,1)S(1)} %maximum_dynamic-update-slice_fusion), kind=kOutput, calls=%fused_computation.22 | convolution fusion | flops 2147745792 | bytes 11010048 | tf_op jit(solution)/shard_map/dot_general | solution.py:219
  56.1 7.0 %collective-permute-done.43 = bf16[128,3072]{1,0:T(8,128)(2,1)S(1)} collective-permute-done((bf16[128,3072]{1,0:T(8,128)(2,1)S(1)}, bf16[128,3072]{1,0:T(8,128)(2,1)S(1)}, u32[]{:S(2)}, u32[]{:S(2)}) %collective-permute-start.43) | collective-permute-done | bytes 786464 | tf_op jit(solution)/shard_map/ppermute | solution.py:106
  72.7 7.6 %collective-permute-done.8 = bf16[256,256]{1,0:T(8,128)(2,1)S(1)} collective-permute-done((bf16[256,256]{1,0:T(8,128)(2,1)S(1)}, bf16[256,256]{1,0:T(8,128)(2,1)S(1)}, u32[]{:S(2)}, u32[]{:S(2)}) %collective-permute-start.8) | collective-permute-done | bytes 131104 | tf_op jit(solution)/shard_map/ppermute | solution.py:100
  82.5 2.5 %collective-permute-done.9 = bf16[128,256]{1,0:T(8,128)(2,1)S(1)} collective-permute-done((bf16[128,256]{1,0:T(8,128)(2,1)S(1)}, bf16[128,256]{1,0:T(8,128)(2,1)S(1)}, u32[]{:S(2)}, u32[]{:S(2)}) %collective-permute-start.9) | collective-permute-done | bytes 65568 | tf_op jit(solution)/shard_map/ppermute | solution.py:100
  88.3 2.4 %collective-permute-start.31 = (bf16[32,2048]{1,0:T(8,128)(2,1)S(1)}, bf16[32,2048]{1,0:T(8,128)(2,1)S(1)}, u32[]{:S(2)}, u32[]{:S(2)}) collective-permute-start(bf16[32,2048]{1,0:T(8,128)(2,1)S(1)} %get-tuple-element.44), channel_id=1, source_target_pairs={{0,24},{8,0},{16,8},{24,16},{1,25},{9,1},{17,9},{25,17},{2,26},{10... | collective-permute-start | bytes 393224 | tf_op jit(solution)/shard_map/ppermute | solution.py:106
  91.4 1.9 collective-permute-start.29
  96.2 2.0 %collective-permute-done.17 = bf16[32,512]{1,0:T(8,128)(2,1)S(1)} collective-permute-done((bf16[32,512]{1,0:T(8,128)(2,1)S(1)}, bf16[32,512]{1,0:T(8,128)(2,1)S(1)}, u32[]{:S(2)}, u32[]{:S(2)}) %collective-permute-start.17) | collective-permute-done | bytes 32800 | tf_op jit(solution)/shard_map/ppermute | solution.py:106
  98.2 22.5 %collective-permute-start.44 = (bf16[128,3072]{1,0:T(8,128)(2,1)S(1)}, bf16[128,3072]{1,0:T(8,128)(2,1)S(1)}, u32[]{:S(2)}, u32[]{:S(2)}) collective-permute-start(bf16[128,3072]{1,0:T(8,128)(2,1)S(1)} %collective-permute-done.43), channel_id=1, source_target_pairs={{0,8},{8,16},{16,24},{24,0},{1,9},{9,17},{17,25},{25,1},{2,10},{10... | collective-permute-start | bytes 2359304 | tf_op jit(solution)/shard_map/ppermute | solution.py:106
  120.7 15.7 %collective-permute-done.15 = bf16[32,512]{1,0:T(8,128)(2,1)S(1)} collective-permute-done((bf16[32,512]{1,0:T(8,128)(2,1)S(1)}, bf16[32,512]{1,0:T(8,128)(2,1)S(1)}, u32[]{:S(2)}, u32[]{:S(2)}) %collective-permute-start.15) | collective-permute-done | bytes 32800 | tf_op jit(solution)/shard_map/ppermute | solution.py:106
  140.1 3.5 %collective-permute-start.34 = (bf16[32,2048]{1,0:T(8,128)(2,1)S(1)}, bf16[32,2048]{1,0:T(8,128)(2,1)S(1)}, u32[]{:S(2)}, u32[]{:S(2)}) collective-permute-start(bf16[32,2048]{1,0:T(8,128)(2,1)S(1)} %get-tuple-element.35), channel_id=1, source_target_pairs={{0,24},{8,0},{16,8},{24,16},{1,25},{9,1},{17,9},{25,17},{2,26},{10... | collective-permute-start | bytes 393224 | tf_op jit(solution)/shard_map/ppermute | solution.py:106
  143.5 2.6 %collective-permute-start.32 = (bf16[32,2048]{1,0:T(8,128)(2,1)S(1)}, bf16[32,2048]{1,0:T(8,128)(2,1)S(1)}, u32[]{:S(2)}, u32[]{:S(2)}) collective-permute-start(bf16[32,2048]{1,0:T(8,128)(2,1)S(1)} %get-tuple-element.35), channel_id=1, source_target_pairs={{0,16},{8,24},{16,0},{24,8},{1,17},{9,25},{17,1},{25,9},{2,18},{10... | collective-permute-start | bytes 393224 | tf_op jit(solution)/shard_map/ppermute | solution.py:106
  150.4 11.1 %collective-permute-done.32 = bf16[32,2048]{1,0:T(8,128)(2,1)S(1)} collective-permute-done((bf16[32,2048]{1,0:T(8,128)(2,1)S(1)}, bf16[32,2048]{1,0:T(8,128)(2,1)S(1)}, u32[]{:S(2)}, u32[]{:S(2)}) %collective-permute-start.32) | collective-permute-done | bytes 131104 | tf_op jit(solution)/shard_map/ppermute | solution.py:106
  170.3 2.8 %collective-permute-done.36 = f32[1,2]{1,0:T(1,128)S(1)} collective-permute-done((f32[1,2]{1,0:T(1,128)S(1)}, f32[1,2]{1,0:T(1,128)S(1)}, u32[]{:S(2)}, u32[]{:S(2)}) %collective-permute-start.36) | collective-permute-done | bytes 40 | tf_op jit(solution)/shard_map/ppermute | solution.py:100
  175.8 2.2 %collective-permute-done.37 = f32[1,2]{1,0:T(1,128)S(1)} collective-permute-done((f32[1,2]{1,0:T(1,128)S(1)}, f32[1,2]{1,0:T(1,128)S(1)}, u32[]{:S(2)}, u32[]{:S(2)}) %collective-permute-start.37) | collective-permute-done | bytes 40 | tf_op jit(solution)/shard_map/ppermute | solution.py:100
  185.3 4.1 %shard_map.179 = (f32[256,512]{1,0:T(8,128)}, bf16[1024,512]{1,0:T(8,128)(2,1)}) custom-call(s32[1]{0:T(128)} %bitcast.place_ref, f32[1,1]{1,0:T(1,128)S(6)} %rsqrt.8.scale_ref, bf16[1024,512]{1,0:T(8,128)(2,1)} %pad_maximum_fusion.basis_ref, bf16[128,512]{1,0:T(8,128)(2,1)} %copy-done.9, bf16[128,512]{1,0:T(8,128)(2,1)} %copy-done.12, ...), custom_call_target="tpu_custom_call" | custom-call | tf_op jit(solution)/shard_map/pallas_call | solution.py:74
  190.8 6.1 %shard_map.180 = (f32[128,2048]{1,0:T(8,128)}, bf16[512,2048]{1,0:T(8,128)(2,1)}) custom-call(s32[1]{0:T(128)} %bitcast.place_ref, f32[1,1]{1,0:T(1,128)S(6)} %rsqrt.9.scale_ref, bf16[512,512]{1,0:T(8,128)(2,1)} %pad_maximum_fusion.18.basis_ref, bf16[128,2048]{1,0:T(8,128)(2,1)} %copy-done.2, bf16[128,2048]{1,0:T(8,128)(2,1)} %copy-done.5, ...), custom_call_target="tpu_custom_call" | custom-call | tf_op jit(solution)/shard_map/pallas_call | solution.py:74
  (225 shorter events, 73.6 us)
Async XLA Ops:
  7.8 15.8 %collective-permute-start.2 = (bf16[256,256]{1,0:T(8,128)(2,1)S(1)}, bf16[256,256]{1,0:T(8,128)(2,1)S(1)}, u32[]{:S(2)}, u32[]{:S(2)}) collective-permute-start(bf16[256,256]{1,0:T(8,128)(2,1)S(1)} %constant_dynamic-slice_fusion.17), channel_id=1, source_target_pairs={{0,24},{8,0},{16,8},{24,16},{1,25},{9,1},{17,9},{25,17},{2,26},{10... | collective-permute-start | bytes 393224 | tf_op jit(solution)/shard_map/ppermute | solution.py:106
  15.1 14.7 %collective-permute-start.21 = (bf16[512,256]{1,0:T(8,128)(2,1)S(1)}, bf16[512,256]{1,0:T(8,128)(2,1)}, u32[]{:S(2)}, u32[]{:S(2)}) collective-permute-start(bf16[512,256]{1,0:T(8,128)(2,1)S(1)} %get-tuple-element.20), channel_id=1, source_target_pairs={{0,2},{2,0},{4,6},{6,4},{1,3},{3,1},{5,7},{7,5},{8,10},{10,8},{12,... | collective-permute-start | bytes 786440 | tf_op jit(solution)/shard_map/ppermute | solution.py:100
  21.9 12.1 %collective-permute-start.22 = (bf16[512,256]{1,0:T(8,128)(2,1)S(1)}, bf16[512,256]{1,0:T(8,128)(2,1)}, u32[]{:S(2)}, u32[]{:S(2)}) collective-permute-start(bf16[512,256]{1,0:T(8,128)(2,1)S(1)} %get-tuple-element.20), channel_id=1, source_target_pairs={{0,4},{2,6},{4,0},{6,2},{1,5},{3,7},{5,1},{7,3},{8,12},{10,14},{12... | collective-permute-start | bytes 786440 | tf_op jit(solution)/shard_map/ppermute | solution.py:100
  23.5 12.2 %collective-permute-start.23 = (bf16[512,256]{1,0:T(8,128)(2,1)S(1)}, bf16[512,256]{1,0:T(8,128)(2,1)}, u32[]{:S(2)}, u32[]{:S(2)}) collective-permute-start(bf16[512,256]{1,0:T(8,128)(2,1)S(1)} %get-tuple-element.20), channel_id=1, source_target_pairs={{0,6},{2,4},{4,2},{6,0},{1,7},{3,5},{5,3},{7,1},{8,14},{10,12},{12... | collective-permute-start | bytes 786440 | tf_op jit(solution)/shard_map/ppermute | solution.py:100
  27.7 15.1 %collective-permute-start.3 = (bf16[1024,256]{1,0:T(8,128)(2,1)S(1)}, bf16[1024,256]{1,0:T(8,128)(2,1)S(1)}, u32[]{:S(2)}, u32[]{:S(2)}) collective-permute-start(bf16[1024,256]{1,0:T(8,128)(2,1)S(1)} %get-tuple-element.16), channel_id=1, source_target_pairs={{0,2},{2,0},{4,6},{6,4},{1,3},{3,1},{5,7},{7,5},{8,10},{10,8},{12,... | collective-permute-start | bytes 1572872 | tf_op jit(solution)/shard_map/ppermute | solution.py:100
  28.2 15.7 %collective-permute-start.4 = (bf16[1024,256]{1,0:T(8,128)(2,1)S(1)}, bf16[1024,256]{1,0:T(8,128)(2,1)S(1)}, u32[]{:S(2)}, u32[]{:S(2)}) collective-permute-start(bf16[1024,256]{1,0:T(8,128)(2,1)S(1)} %get-tuple-element.16), channel_id=1, source_target_pairs={{0,4},{2,6},{4,0},{6,2},{1,5},{3,7},{5,1},{7,3},{8,12},{10,14},{12... | collective-permute-start | bytes 1572872 | tf_op jit(solution)/shard_map/ppermute | solution.py:100
  41.4 21.8 %collective-permute-start.43 = (bf16[128,3072]{1,0:T(8,128)(2,1)S(1)}, bf16[128,3072]{1,0:T(8,128)(2,1)S(1)}, u32[]{:S(2)}, u32[]{:S(2)}) collective-permute-start(bf16[128,3072]{1,0:T(8,128)(2,1)S(1)} %pad_maximum_fusion.1), channel_id=1, source_target_pairs={{0,8},{8,16},{16,24},{24,0},{1,9},{9,17},{17,25},{25,1},{2,10},{10... | collective-permute-start | bytes 2359304 | tf_op jit(solution)/shard_map/ppermute | solution.py:106
  48.8 17.0 %collective-permute-start.25 = (bf16[256,1024]{1,0:T(8,128)(2,1)S(1)}, bf16[256,1024]{1,0:T(8,128)(2,1)S(1)}, u32[]{:S(2)}, u32[]{:S(2)}) collective-permute-start(bf16[256,1024]{1,0:T(8,128)(2,1)S(1)} %fusion.14), channel_id=1, source_target_pairs={{0,2},{2,0},{4,6},{6,4},{1,3},{3,1},{5,7},{7,5},{8,10},{10,8},{12,... | collective-permute-start | bytes 1572872 | tf_op jit(solution)/shard_map/ppermute | solution.py:100
  50.2 18.0 %collective-permute-start.27 = (bf16[256,1024]{1,0:T(8,128)(2,1)S(1)}, bf16[256,1024]{1,0:T(8,128)(2,1)S(1)}, u32[]{:S(2)}, u32[]{:S(2)}) collective-permute-start(bf16[256,1024]{1,0:T(8,128)(2,1)S(1)} %fusion.17), channel_id=1, source_target_pairs={{0,4},{2,6},{4,0},{6,2},{1,5},{3,7},{5,1},{7,3},{8,12},{10,14},{12... | collective-permute-start | bytes 1572872 | tf_op jit(solution)/shard_map/ppermute | solution.py:100
  55.6 13.5 %collective-permute-start.7 = (bf16[1024,256]{1,0:T(8,128)(2,1)S(1)}, bf16[1024,256]{1,0:T(8,128)(2,1)S(1)}, u32[]{:S(2)}, u32[]{:S(2)}) collective-permute-start(bf16[1024,256]{1,0:T(8,128)(2,1)S(1)} %fusion.20), channel_id=1, source_target_pairs={{0,1},{1,0},{2,3},{3,2},{4,5},{5,4},{6,7},{7,6},{8,9},{9,8},{10,11... | collective-permute-start | bytes 1572872 | tf_op jit(solution)/shard_map/ppermute | solution.py:103
  55.6 17.0 %collective-permute-start.38 = (bf16[1024,256]{1,0:T(8,128)(2,1)S(1)}, bf16[1024,256]{1,0:T(8,128)(2,1)S(1)}, u32[]{:S(2)}, u32[]{:S(2)}) collective-permute-start(bf16[1024,256]{1,0:T(8,128)(2,1)S(1)} %get-tuple-element.16), channel_id=1, source_target_pairs={{0,1},{1,0},{2,3},{3,2},{4,5},{5,4},{6,7},{7,6},{8,9},{9,8},{10,11... | collective-permute-start | bytes 1572872 | tf_op jit(solution)/shard_map/ppermute | solution.py:103
  66.6 21.5 %collective-permute-start.26 = (bf16[128,1024]{1,0:T(8,128)(2,1)S(1)}, bf16[128,1024]{1,0:T(8,128)(2,1)S(1)}, u32[]{:S(2)}, u32[]{:S(2)}) collective-permute-start(bf16[128,1024]{1,0:T(8,128)(2,1)S(1)} %slice.197), channel_id=1, source_target_pairs={{0,4},{2,6},{4,0},{6,2},{1,5},{3,7},{5,1},{7,3},{8,12},{10,14},{12... | collective-permute-start | bytes 786440 | tf_op jit(solution)/shard_map/ppermute | solution.py:100
  69.0 19.2 %collective-permute-start.28 = (bf16[128,1024]{1,0:T(8,128)(2,1)S(1)}, bf16[128,1024]{1,0:T(8,128)(2,1)S(1)}, u32[]{:S(2)}, u32[]{:S(2)}) collective-permute-start(bf16[128,1024]{1,0:T(8,128)(2,1)S(1)} %slice.196), channel_id=1, source_target_pairs={{0,2},{2,0},{4,6},{6,4},{1,3},{3,1},{5,7},{7,5},{8,10},{10,8},{12,... | collective-permute-start | bytes 786440 | tf_op jit(solution)/shard_map/ppermute | solution.py:100
  88.3 49.4 %collective-permute-start.31 = (bf16[32,2048]{1,0:T(8,128)(2,1)S(1)}, bf16[32,2048]{1,0:T(8,128)(2,1)S(1)}, u32[]{:S(2)}, u32[]{:S(2)}) collective-permute-start(bf16[32,2048]{1,0:T(8,128)(2,1)S(1)} %get-tuple-element.44), channel_id=1, source_target_pairs={{0,24},{8,0},{16,8},{24,16},{1,25},{9,1},{17,9},{25,17},{2,26},{10... | collective-permute-start | bytes 393224 | tf_op jit(solution)/shard_map/ppermute | solution.py:106
  90.8 48.3 %collective-permute-start.30 = (bf16[32,2048]{1,0:T(8,128)(2,1)S(1)}, bf16[32,2048]{1,0:T(8,128)(2,1)S(1)}, u32[]{:S(2)}, u32[]{:S(2)}) collective-permute-start(bf16[32,2048]{1,0:T(8,128)(2,1)S(1)} %get-tuple-element.43), channel_id=1, source_target_pairs={{0,16},{8,24},{16,0},{24,8},{1,17},{9,25},{17,1},{25,9},{2,18},{10... | collective-permute-start | bytes 393224 | tf_op jit(solution)/shard_map/ppermute | solution.py:106
  91.4 47.7 %collective-permute-start.29 = (bf16[32,2048]{1,0:T(8,128)(2,1)S(1)}, bf16[32,2048]{1,0:T(8,128)(2,1)S(1)}, u32[]{:S(2)}, u32[]{:S(2)}) collective-permute-start(bf16[32,2048]{1,0:T(8,128)(2,1)S(1)} %get-tuple-element.42), channel_id=1, source_target_pairs={{0,8},{8,16},{16,24},{24,0},{1,9},{9,17},{17,25},{25,1},{2,10},{10... | collective-permute-start | bytes 393224 | tf_op jit(solution)/shard_map/ppermute | solution.py:106
  95.9 24.8 %collective-permute-start.16 = (bf16[32,512]{1,0:T(8,128)(2,1)S(1)}, bf16[32,512]{1,0:T(8,128)(2,1)S(1)}, u32[]{:S(2)}, u32[]{:S(2)}) collective-permute-start(bf16[32,512]{1,0:T(8,128)(2,1)S(1)} %get-tuple-element.32), channel_id=1, source_target_pairs={{0,8},{8,16},{16,24},{24,0},{1,9},{9,17},{17,25},{25,1},{2,10},{10... | collective-permute-start | bytes 98312 | tf_op jit(solution)/shard_map/ppermute | solution.py:106
  98.2 63.5 %collective-permute-start.44 = (bf16[128,3072]{1,0:T(8,128)(2,1)S(1)}, bf16[128,3072]{1,0:T(8,128)(2,1)S(1)}, u32[]{:S(2)}, u32[]{:S(2)}) collective-permute-start(bf16[128,3072]{1,0:T(8,128)(2,1)S(1)} %collective-permute-done.43), channel_id=1, source_target_pairs={{0,8},{8,16},{16,24},{24,0},{1,9},{9,17},{17,25},{25,1},{2,10},{10... | collective-permute-start | bytes 2359304 | tf_op jit(solution)/shard_map/ppermute | solution.py:106
  120.7 15.8 %collective-permute-start.15 = (bf16[32,512]{1,0:T(8,128)(2,1)S(1)}, bf16[32,512]{1,0:T(8,128)(2,1)S(1)}, u32[]{:S(2)}, u32[]{:S(2)}) collective-permute-start(bf16[32,512]{1,0:T(8,128)(2,1)S(1)} %get-tuple-element.32), channel_id=1, source_target_pairs={{0,16},{8,24},{16,0},{24,8},{1,17},{9,25},{17,1},{25,9},{2,18},{10... | collective-permute-start | bytes 98312 | tf_op jit(solution)/shard_map/ppermute | solution.py:106
  143.5 17.9 %collective-permute-start.32 = (bf16[32,2048]{1,0:T(8,128)(2,1)S(1)}, bf16[32,2048]{1,0:T(8,128)(2,1)S(1)}, u32[]{:S(2)}, u32[]{:S(2)}) collective-permute-start(bf16[32,2048]{1,0:T(8,128)(2,1)S(1)} %get-tuple-element.35), channel_id=1, source_target_pairs={{0,16},{8,24},{16,0},{24,8},{1,17},{9,25},{17,1},{25,9},{2,18},{10... | collective-permute-start | bytes 393224 | tf_op jit(solution)/shard_map/ppermute | solution.py:106
  148.0 36.6 %collective-permute-start.41 = (bf16[128,256]{1,0:T(8,128)(2,1)S(1)}, bf16[128,256]{1,0:T(8,128)(2,1)S(1)}, u32[]{:S(2)}, u32[]{:S(2)}) collective-permute-start(bf16[128,256]{1,0:T(8,128)(2,1)S(1)} %slice.152), channel_id=1, source_target_pairs={{0,2},{2,0},{4,6},{6,4},{1,3},{3,1},{5,7},{7,5},{8,10},{10,8},{12,... | collective-permute-start | bytes 196616 | tf_op jit(solution)/shard_map/ppermute | solution.py:100
  161.7 21.3 %collective-permute-start.45 = (bf16[128,3072]{1,0:T(8,128)(2,1)S(1)}, bf16[128,3072]{1,0:T(8,128)(2,1)S(1)}, u32[]{:S(2)}, u32[]{:S(2)}) collective-permute-start(bf16[128,3072]{1,0:T(8,128)(2,1)S(1)} %collective-permute-done.44), channel_id=1, source_target_pairs={{0,8},{8,16},{16,24},{24,0},{1,9},{9,17},{17,25},{25,1},{2,10},{10... | collective-permute-start | bytes 2359304 | tf_op jit(solution)/shard_map/ppermute | solution.py:106
  161.8 20.4 %collective-permute-start.47 = (bf16[128,2048]{1,0:T(8,128)(2,1)S(1)}, bf16[128,2048]{1,0:T(8,128)(2,1)S(1)}, u32[]{:S(2)}, u32[]{:S(2)}) collective-permute-start(bf16[128,2048]{1,0:T(8,128)(2,1)S(1)} %fusion.31.refs_0_), channel_id=1, source_target_pairs={{0,2},{2,0},{4,6},{6,4},{1,3},{3,1},{5,7},{7,5},{8,10},{10,8},{12,... | collective-permute-start | bytes 1572872 | tf_op jit(solution)/shard_map/ppermute | solution.py:100
  163.2 18.2 %collective-permute-start.48 = (bf16[128,2048]{1,0:T(8,128)(2,1)S(1)}, bf16[128,2048]{1,0:T(8,128)(2,1)S(1)}, u32[]{:S(2)}, u32[]{:S(2)}) collective-permute-start(bf16[128,2048]{1,0:T(8,128)(2,1)S(1)} %fusion.31.refs_0_), channel_id=1, source_target_pairs={{0,4},{2,6},{4,0},{6,2},{1,5},{3,7},{5,1},{7,3},{8,12},{10,14},{12... | collective-permute-start | bytes 1572872 | tf_op jit(solution)/shard_map/ppermute | solution.py:100
  (52 other events, 496.9 us)
where the time goes:
time: 197 us
  starting transfers between devices  78.1 us (40%)
  waiting for transfers between devices  64.6 us (33%)
  local copies, waits for them, and re-layouts  16.4 us (8%)
  other arithmetic  14.9 us (8%)
  Pallas kernels  10.1 us (5%)
  matrix products  9.93 us (5%)
  between operations  2.89 us (1%)
    ppermute x21, starting transfers between devices, shift(): return lax.ppermute(value, 'fs', [(k, (k + step) % nf) for k in range(nf)])  52.5 us
    ppermute x21, waiting for transfers between devices, shift(): return lax.ppermute(value, 'fs', [(k, (k + step) % nf) for k in range(nf)])  43.4 us
    ppermute x25, starting transfers between devices, flip(): return lax.ppermute(value, 'rep', [(k, k ^ bits) for k in range(nr)])  25.1 us
    ppermute x25, waiting for transfers between devices, flip(): return lax.ppermute(value, 'rep', [(k, k ^ bits) for k in range(nr)])  20.8 us
    pallas_call x2, Pallas kernels, finish(): pl.pallas_call(functools.partial(finish_kernel, nf, nr, 1, rows), grid_sp...  10.1 us
    dynamic_update_slice x5, local copies, waits for them, and re-layouts, by_rep(): whole = lax.dynamic_update_slice(whole, value, ((rep ^ bits) * rows, 0))  5.09 us
    dot_general x8, matrix products, dot_rows(): lax.dot_general(left, right, (((0,), (0,)), ((), ())), preferred_element_...  4.29 us
    unnamed x50, local copies, waits for them, and re-layouts  4.03 us
  transfers between devices with their start and end apart: 51, of which 18 were waited for; matrix products, arithmetic and copies ran while one was open for 18% of the time, Pallas kernels for 2%

commit v1 on v0

v1 whole, which is shorter than its diff:
```python
import functools

import jax
import jax.numpy as jnp
from jax import lax
from jax.experimental import pallas as pl
from jax.experimental.pallas import tpu as pltpu
from jax.sharding import PartitionSpec as P


beta_first = 0.6
beta_second = 0.8
step_rate = 0.01
small_eps = 1e-06

f32 = jnp.float32
bf16 = jnp.bfloat16
whole_vmem = pl.BlockSpec(memory_space=pltpu.VMEM)


def dot_rows(left, right):
    return lax.dot_general(left, right, (((0,), (0,)), ((), ())), preferred_element_type=f32)


def after(value, *others):
    return lax.optimization_barrier((value, *others))[0]


def natural_kernel(nf, squares, place_ref, *refs):
    blocks, refs = refs[:nf], refs[nf:]
    before, out_ref = refs[:-2] if squares else (), refs[-2 if squares else -1]
    rows = blocks[0].shape[0]
    for s in range(nf):
        source = lax.rem(place_ref[0] + (nf - s), nf)
        out_ref[pl.ds(pl.multiple_of(source * rows, rows), rows), :] = blocks[s][...]
    if squares:
        total = jnp.zeros((out_ref.shape[0], 128), f32)
        for at in range(0, out_ref.shape[1], 128):
            wide = out_ref[:, at : at + 128].astype(f32)
            total = total + wide * wide
        total = jnp.sum(total.reshape(-1, 8, 128), axis=0)
        refs[-1][...] = jnp.concatenate([part[...] for part in before] + [total], axis=0)


def natural(place, blocks, squares=False, before=()):
    nf = len(blocks)
    rows, columns = blocks[0].shape
    out_shape = [jax.ShapeDtypeStruct((nf * rows, columns), blocks[0].dtype)]
    if squares:
        out_shape.append(jax.ShapeDtypeStruct((8 * (len(before) + 1), 128), f32))
    out = pl.pallas_call(
        functools.partial(natural_kernel, nf, squares),
        in_specs=[pl.BlockSpec(memory_space=pltpu.SMEM)] + [whole_vmem] * (nf + len(before)),
        out_specs=[whole_vmem] * len(out_shape),
        out_shape=out_shape,
        compiler_params=pltpu.CompilerParams(vmem_limit_bytes=8 * 2**20),
    )(place.reshape(1), *blocks, *before)
    return out if squares else out[0]


def finish_kernel(nf, nr, fold, rows, count, first, place_ref, *refs):
    sums, basis_ref, refs = refs[:nr], refs[nr], refs[nr + 1 :]
    pieces, weights = refs[: nr + 1], refs[nr + 1 : nr + 1 + nf * fold]
    update_ref, copy_ref, spread_ref, product_ref = refs[nr + 1 + nf * fold :]
    step, steps = pl.program_id(0), pl.num_programs(0)
    depth = pieces[0].shape[0]
    for k in range(nr - 1):
        spread_ref[k * depth : (k + 1) * depth, :] = pieces[k][...]

    @pl.when(step < steps // 2)
    def _():
        spread_ref[(nr - 1) * depth :, :] = pieces[nr - 1][...]

    @pl.when(step >= steps // 2)
    def _():
        spread_ref[(nr - 1) * depth :, :] = pieces[nr][...]

    total = sum(part[first : first + 8, :] for part in sums)
    scale = lax.rsqrt(jnp.sum(total, keepdims=True) / count + small_eps)
    product = jnp.dot(basis_ref[...], spread_ref[...], preferred_element_type=f32)
    product_ref[...] = scale * product
    part = rows // fold
    for s in range(nf):
        source = lax.rem(place_ref[0] + (nf - s), nf)
        for n in range(fold):
            here = pl.ds(pl.multiple_of(source * rows + n * part, part), part)
            weight = weights[s * fold + n][...].astype(f32)
            copy_ref[here, :] = (weight - step_rate * product_ref[here, :]).astype(bf16)
    mine = pl.ds(pl.multiple_of(place_ref[0] * rows, rows), rows)
    update_ref[...] = product_ref[mine, :]


def finish(nf, nr, nt, place, sums, first, basis, pieces, ring, starts):
    depth, columns = pieces[0].shape
    part, fold = ring[0].shape[0], len(starts)
    rows = part * fold
    steps = 4 if columns % (4 * 256) == 0 else 2
    width = columns // steps
    half = steps // 2
    column = lambda s, p: (0, s)
    whole = lambda s, p: (0, 0)
    weight_specs = [
        pl.BlockSpec((part, width), lambda s, p, at=start // width: (0, at + s))
        for _ in ring
        for start in starts
    ]
    in_specs = [
        *[pl.BlockSpec(part.shape, whole) for part in sums],
        pl.BlockSpec(basis.shape, whole),
        *[pl.BlockSpec((depth, width), column) for _ in range(nr - 1)],
        pl.BlockSpec((depth, width), lambda s, p: (0, jnp.minimum(s, half - 1))),
        pl.BlockSpec((depth, width), lambda s, p: (0, jnp.maximum(s - half, 0))),
        *weight_specs,
    ]
    weights = [value for value in ring for _ in starts]
    return pl.pallas_call(
        functools.partial(finish_kernel, nf, nr, fold, rows, depth * nr * columns * nt, first),
        grid_spec=pltpu.PrefetchScalarGridSpec(
            num_scalar_prefetch=1,
            grid=(steps,),
            in_specs=in_specs,
            out_specs=[
                pl.BlockSpec((rows, width), column),
                pl.BlockSpec((nf * rows, width), column),
            ],
            scratch_shapes=[
                pltpu.VMEM((nr * depth, width), bf16),
                pltpu.VMEM((nf * rows, width), f32),
            ],
        ),
        out_shape=[
            jax.ShapeDtypeStruct((rows, columns), f32),
            jax.ShapeDtypeStruct((nf * rows, columns), bf16),
        ],
        compiler_params=pltpu.CompilerParams(vmem_limit_bytes=20 * 2**20),
    )(place.reshape(1), *sums, basis, *pieces, *weights)


def make_body(nf, nr, nt):
    assert nr == 4 and nt == 2

    def flip(value, bits):
        return lax.ppermute(value, "rep", [(k, k ^ bits) for k in range(nr)])

    def swap(value):
        return lax.ppermute(value, "tp", [(0, 1), (1, 0)])

    def shift(value, step):
        return lax.ppermute(value, "fs", [(k, (k + step) % nf) for k in range(nf)])

    def body(
        query_input,
        query_cotangent,
        branch_output,
        layer_cotangent,
        query_weight,
        output_weight,
        query_basis,
        output_basis,
        query_first,
        query_second,
        output_first,
        output_second,
    ):
        place = lax.axis_index("fs")
        rep = lax.axis_index("rep")
        core = lax.axis_index("tp")
        place, rep, core = lax.optimization_barrier((place, rep, core))
        low, high = rep % 2, rep // 2
        mine = high == core

        def relative(own, other):
            kept, sent = lax.select_n(mine, other, own), lax.select_n(mine, own, other)
            quarter = kept.shape[1] // 2
            rows = kept.shape[0]

            def part(value, bit):
                return lax.dynamic_slice(value, (0, bit * quarter), (rows, quarter))

            return [part(kept, low), part(kept, 1 - low), part(sent, low), part(sent, 1 - low)]

        def half_basis(basis):
            half = basis.shape[1] // nt
            return lax.dynamic_slice(basis, (0, core * half), (basis.shape[0], half))

        def along_fs(value):
            return [value] + [shift(value, s) for s in range(1, nf)]

        def sum_blocks(inputs, blocks):
            width = inputs.shape[1] // nr
            total = None
            for bits, pieces in blocks:
                at = (rep ^ bits) * width
                for piece in pieces:
                    depth = piece.shape[0]
                    columns = lax.dynamic_slice(inputs, (0, at), (inputs.shape[0], depth))
                    more = jnp.dot(columns, piece, preferred_element_type=f32)
                    total = more if total is None else total + more
                    at = at + depth
            return total.astype(bf16)

        def project(inner, other, cotangent):
            here, by_x, by_y, far = relative(inner, other)
            half = cotangent.shape[1] // 2
            left, right = cotangent[:, :half], cotangent[:, half:]
            block = here.shape[1]
            both = lambda a, b: jnp.concatenate([a, b], axis=1)
            sent = dot_rows(both(by_x, far), left).astype(bf16)
            sent_other = dot_rows(both(by_y, far), right).astype(bf16)
            got = flip(sent, 1).astype(f32)
            got_other = flip(sent_other, 2).astype(f32)
            first_on = (dot_rows(by_y, left) + got[block:]).astype(bf16)
            second_on = (dot_rows(by_x, right) + got_other[block:]).astype(bf16)
            first_more = flip(first_on, 2).astype(f32)
            second_more = flip(second_on, 1).astype(f32)
            first = dot_rows(here, left) + got[:block] + first_more
            second = dot_rows(here, right) + got_other[:block] + second_more
            total = jnp.concatenate([first, second], axis=1)
            rows = block // nf

            def rows_of(step):
                at = (place + step) % nf * rows
                return lax.dynamic_slice(total, (at, 0), (rows, total.shape[1]))

            arrived = [shift(rows_of(s).astype(bf16), s) for s in range(1, nf)]
            projected = rows_of(0)
            for value in arrived:
                projected = projected + value.astype(f32)
            return projected, sent_other, second_on

        def moments(first, second, projected):
            first_next = beta_first * first + (1.0 - beta_first) * projected
            second_next = beta_second * second + (1.0 - beta_second) * projected * projected
            rounded = (first_next / jnp.sqrt(second_next)).astype(bf16)
            return first_next, second_next, rounded

        basis_o = natural(place, along_fs(half_basis(output_basis)))
        basis_q = natural(place, along_fs(half_basis(query_basis)))
        x_o, y_o, d_o = flip(basis_o, 1), flip(basis_o, 2), flip(basis_o, 3)
        x_q, y_q = flip(basis_q, 1), flip(basis_q, 2)
        inner_o = sum_blocks(branch_output, [(0, [basis_o]), (1, [x_o]), (2, [y_o]), (3, [d_o])])
        projected_o, sent_o, on_o = project(inner_o, swap(inner_o), layer_cotangent)
        x_q, y_q = lax.optimization_barrier((x_q, y_q, sent_o))[:2]
        split = basis_q.shape[0] // 2
        far_q = [flip(y_q[:split], 1), flip(x_q[split:], 2)]
        far_q = lax.optimization_barrier((*far_q, on_o))[:2]
        inner_q = sum_blocks(query_input, [(0, [basis_q]), (1, [x_q]), (2, [y_q]), (3, far_q)])
        projected_q = project(inner_q, swap(inner_q), query_cotangent)[0]

        fold = query_weight.shape[0] // output_weight.shape[0]
        rows_o, columns_o = output_weight.shape
        columns_q = query_weight.shape[1]
        packed = [output_weight] + [
            query_weight[n * rows_o : (n + 1) * rows_o] for n in range(fold)
        ]
        ring = [after(jnp.concatenate(packed, axis=1).astype(bf16), basis_q)]

        def turn():
            ring.append(shift(ring[-1], 1))

        late_o, late_q = lax.optimization_barrier((basis_o, basis_q, inner_q))[:2]
        order_o = jnp.concatenate(relative(late_o, swap(late_o)), axis=1)
        order_q = jnp.concatenate(relative(late_q, swap(late_q)), axis=1)

        first_o, second_o, rounded_o = moments(output_first, output_second, projected_o)
        first_q, second_q, rounded_q = moments(query_first, query_second, projected_q)
        block_o, sums_o = natural(place, along_fs(rounded_o), True)
        blocks_q = lax.optimization_barrier((*along_fs(rounded_q), block_o))[:-1]
        block_q, sums = natural(place, blocks_q, True, (sums_o,))

        for n in range(1, nf):
            if n == nf - 1:
                ring[-1] = after(ring[-1], block_o)
            turn()

        sums = sums + swap(sums)
        sums = [sums, flip(sums, 1), flip(sums, 2), flip(sums, 3)]

        def spread(block, x, y):
            cut = block.shape[1] // 2
            return [block, x, y, flip(y[:, :cut], 1), flip(x[:, cut:], 2)]

        x_o, y_o = flip(block_o, 1), flip(block_o, 2)
        x_q, y_q = flip(block_q, 1), flip(block_q, 2)
        spread_o = spread(block_o, x_o, y_o)
        spread_q = spread(block_q, x_q, y_q)
        starts_q = [columns_o + n * columns_q for n in range(fold)]

        def end(first, order, pieces, starts):
            return finish(nf, nr, nt, place, sums, first, order, pieces, ring, starts)

        update_q, copy_q = end(8, order_q, spread_q, starts_q)
        update_o, copy_o = end(0, order_o, spread_o, [0])
        return (update_q, update_o, first_q, second_q, first_o, second_o, copy_q, copy_o)

    return body


def solution(mesh):
    tokens, columns = P(("fs", "rep"), None), P(("fs", "rep"), "tp")
    rows, both = P(("rep", "fs"), None), P(("rep", "fs"), "tp")
    in_specs = (tokens, columns, tokens, columns, both, both, rows, rows, both, both, both, both)
    out_specs = (both,) * 6 + (P("rep", "tp"),) * 2
    nf = mesh.shape["fs"]
    body = make_body(nf, mesh.shape["rep"], mesh.shape["tp"])

    return jax.shard_map(body, mesh=mesh, in_specs=in_specs, out_specs=out_specs, check_vma=False)
```

time: 197 us -> 190 us (0.964)
  local copies, waits for them, and re-layouts: 16.4 us -> 2.24 us
  starting transfers between devices: 78.1 us -> 86.7 us
  other arithmetic: 14.9 us -> 8.89 us
  matrix products: 9.93 us -> 15 us
  waiting for transfers between devices: 64.6 us -> 69 us
  Pallas kernels: 10.1 us -> 6.9 us
    ppermute x25 -> x26, waiting for transfers between devices: 20.8 us -> 43.6 us  [flip(): return lax.ppermute(value, 'rep', [(k, k ^ bits) for k in range(nr)])]
    ppermute x21, waiting for transfers between devices: 43.4 us -> 24.2 us  [shift(): return lax.ppermute(value, 'fs', [(k, (k + step) % nf) for k in range(nf)])]
    ppermute x25 -> x26, starting transfers between devices: 25.1 us -> 31.6 us  [flip(): return lax.ppermute(value, 'rep', [(k, k ^ bits) for k in range(nr)])]
    dynamic_update_slice x5 -> x0, local copies, waits for them, and re-layouts: 5.09 us -> none  [by_rep(): whole = lax.dynamic_update_slice(whole, value, ((rep ^ bits) * rows, 0))]
    dot_general x2 -> x9, matrix products: 5.64 us -> 9.88 us  [sum_blocks(): more = jnp.dot(columns, piece, preferred_element_type=f32)]
    slice x13 -> x0, local copies, waits for them, and re-layouts: 4.09 us -> none  [the longest x4 3.35 us: body(): weights_o = [value[:, :columns_o] for value in ring]]
    concatenate x4 -> x0, other arithmetic: 3.66 us -> none  [the longest x3 2.3 us: body(): jnp.concatenate([value[:, columns_o + n * columns_q:columns_o + (n + 1) *...]
    pallas_call x2 -> x6, Pallas kernels: 10.1 us -> 6.9 us  [the longest x2 6.63 us: finish(): pl.pallas_call(functools.partial(finish_kernel, nf, nr, fold, rows, depth...]
  transfers between devices with their start and end apart: 51 -> 52, of which waited for: 18 -> 25; matrix products, arithmetic and copies ran while one was open for 18% -> 13% of each run, Pallas kernels for 2% -> 2%
where the time goes in v1:
time: 190 us
  starting transfers between devices  86.7 us (46%)
  waiting for transfers between devices  69 us (36%)
  matrix products  15 us (8%)
  other arithmetic  8.89 us (5%)
  Pallas kernels  6.9 us (4%)
  local copies, waits for them, and re-layouts  2.24 us (1%)
    ppermute x21, starting transfers between devices, shift(): return lax.ppermute(value, 'fs', [(k, (k + step) % nf) for k in range(nf)])  54.9 us
    ppermute x26, waiting for transfers between devices, flip(): return lax.ppermute(value, 'rep', [(k, k ^ bits) for k in range(nr)])  43.6 us
    ppermute x26, starting transfers between devices, flip(): return lax.ppermute(value, 'rep', [(k, k ^ bits) for k in range(nr)])  31.6 us
    ppermute x21, waiting for transfers between devices, shift(): return lax.ppermute(value, 'fs', [(k, (k + step) % nf) for k in range(nf)])  24.2 us
    dot_general x9, matrix products, sum_blocks(): more = jnp.dot(columns, piece, preferred_element_type=f32)  9.88 us
    pallas_call x2, Pallas kernels, finish(): pl.pallas_call(functools.partial(finish_kernel, nf, nr, fold, rows, depth...  6.63 us
    dot_general x12, matrix products, dot_rows(): lax.dot_general(left, right, (((0,), (0,)), ((), ())), preferred_element_...  5.13 us
  transfers between devices with their start and end apart: 52, of which 25 were waited for; matrix products, arithmetic and copies ran while one was open for 13% of the time, Pallas kernels for 2%

profile of v1, /device:TPU:0, one launch (start us, length us, event | category | flops | bytes accessed | tf_op | source)
XLA Modules:
  0.0 190.1 jit_solution(7141038192958591366)
XLA Ops:
  1.5 3.1 %collective-permute-start.5 = (bf16[128,256]{1,0:T(8,128)(2,1)S(1)}, bf16[128,256]{1,0:T(8,128)(2,1)S(1)}, u32[]{:S(2)}, u32[]{:S(2)}) collective-permute-start(bf16[128,256]{1,0:T(8,128)(2,1)S(1)} %constant_dynamic-slice_fusion.14.refs_0_), channel_id=1, source_target_pairs={{0,8},{8,16},{16,24},{24,0},{1,9},{9,17},{17,25},{25,1},{2,10},{10... | collective-permute-start | bytes 196616 | tf_op jit(solution)/shard_map/ppermute | solution.py:149
  4.6 2.6 %collective-permute-start.6 = (bf16[128,256]{1,0:T(8,128)(2,1)S(1)}, bf16[128,256]{1,0:T(8,128)(2,1)S(1)}, u32[]{:S(2)}, u32[]{:S(2)}) collective-permute-start(bf16[128,256]{1,0:T(8,128)(2,1)S(1)} %constant_dynamic-slice_fusion.14.refs_0_), channel_id=1, source_target_pairs={{0,16},{8,24},{16,0},{24,8},{1,17},{9,25},{17,1},{25,9},{2,18},{10... | collective-permute-start | bytes 196616 | tf_op jit(solution)/shard_map/ppermute | solution.py:149
  9.1 2.6 %collective-permute-done.6.refs_2_ = bf16[128,256]{1,0:T(8,128)(2,1)S(1)} collective-permute-done((bf16[128,256]{1,0:T(8,128)(2,1)S(1)}, bf16[128,256]{1,0:T(8,128)(2,1)S(1)}, u32[]{:S(2)}, u32[]{:S(2)}) %collective-permute-start.6) | collective-permute-done | bytes 65568 | tf_op jit(solution)/shard_map/ppermute | solution.py:149
  11.9 2.5 %collective-permute-start.10 = (bf16[512,256]{1,0:T(8,128)(2,1)S(1)}, bf16[512,256]{1,0:T(8,128)(2,1)S(1)}, u32[]{:S(2)}, u32[]{:S(2)}) collective-permute-start(bf16[512,256]{1,0:T(8,128)(2,1)S(1)} %shard_map.180), channel_id=1, source_target_pairs={{0,6},{2,4},{4,2},{6,0},{1,7},{3,5},{5,3},{7,1},{8,14},{10,12},{12... | collective-permute-start | bytes 786440 | tf_op jit(solution)/shard_map/ppermute | solution.py:143
  36.6 7.4 %collective-permute-done.3 = bf16[1024,256]{1,0:T(8,128)(2,1)S(1)} collective-permute-done((bf16[1024,256]{1,0:T(8,128)(2,1)S(1)}, bf16[1024,256]{1,0:T(8,128)(2,1)S(1)}, u32[]{:S(2)}, u32[]{:S(2)}) %collective-permute-start.3) | collective-permute-done | bytes 524320 | tf_op jit(solution)/shard_map/ppermute | solution.py:143
  49.6 2.3 %fusion = f32[1024,256]{1,0:T(8,128)S(1)} fusion(bf16[1024,256]{1,0:T(8,128)(2,1)S(1)} %collective-permute-done.4, bf16[1024,4096]{1,0:T(8,128)(2,1)} %param.12, s32[]{:T(128)S(6)} %select_n.151), kind=kOutput, calls=%fused_computation | convolution fusion | flops 536870912 | bytes 3670020 | tf_op jit(solution)/shard_map/dot_general | solution.py:197
  52.6 3.9 %collective-permute-done.14 = bf16[256,1024]{1,0:T(8,128)(2,1)S(1)} collective-permute-done((bf16[256,1024]{1,0:T(8,128)(2,1)S(1)}, bf16[256,1024]{1,0:T(8,128)(2,1)S(1)}, u32[]{:S(2)}, u32[]{:S(2)}) %collective-permute-start.14) | collective-permute-done | bytes 524320 | tf_op jit(solution)/shard_map/ppermute | solution.py:143
  58.4 3.0 %collective-permute-done.13 = bf16[512,256]{1,0:T(8,128)(2,1)S(1)} collective-permute-done((bf16[512,256]{1,0:T(8,128)(2,1)S(1)}, bf16[512,256]{1,0:T(8,128)(2,1)S(1)}, u32[]{:S(2)}, u32[]{:S(2)}) %collective-permute-start.13) | collective-permute-done | bytes 262176 | tf_op jit(solution)/shard_map/ppermute | solution.py:143
  61.4 4.4 %collective-permute-done.26 = bf16[256,1024]{1,0:T(8,128)(2,1)S(1)} collective-permute-done((bf16[256,1024]{1,0:T(8,128)(2,1)S(1)}, bf16[256,1024]{1,0:T(8,128)(2,1)S(1)}, u32[]{:S(2)}, u32[]{:S(2)}) %collective-permute-start.26) | collective-permute-done | bytes 524320 | tf_op jit(solution)/shard_map/ppermute | solution.py:143
  69.5 3.3 %collective-permute-done.27 = bf16[128,1024]{1,0:T(8,128)(2,1)S(1)} collective-permute-done((bf16[128,1024]{1,0:T(8,128)(2,1)S(1)}, bf16[128,1024]{1,0:T(8,128)(2,1)S(1)}, u32[]{:S(2)}, u32[]{:S(2)}) %collective-permute-start.27) | collective-permute-done | bytes 262176 | tf_op jit(solution)/shard_map/ppermute | solution.py:143
  81.9 2.8 %collective-permute-done.30 = bf16[32,2048]{1,0:T(8,128)(2,1)} collective-permute-done((bf16[32,2048]{1,0:T(8,128)(2,1)}, bf16[32,2048]{1,0:T(8,128)(2,1)}, u32[]{:S(2)}, u32[]{:S(2)}) %collective-permute-start.30) | collective-permute-done | bytes 131104 | tf_op jit(solution)/shard_map/ppermute | solution.py:149
  86.8 23.3 %collective-permute-start.32 = (bf16[32,2048]{1,0:T(8,128)(2,1)S(1)}, bf16[32,2048]{1,0:T(8,128)(2,1)S(1)}, u32[]{:S(2)}, u32[]{:S(2)}) collective-permute-start(bf16[32,2048]{1,0:T(8,128)(2,1)S(1)} %get-tuple-element.54.refs_0_), channel_id=1, source_target_pairs={{0,8},{8,16},{16,24},{24,0},{1,9},{9,17},{17,25},{25,1},{2,10},{10... | collective-permute-start | bytes 393224 | tf_op jit(solution)/shard_map/ppermute | solution.py:149
  110.0 2.4 %collective-permute-start.34 = (bf16[32,2048]{1,0:T(8,128)(2,1)S(1)}, bf16[32,2048]{1,0:T(8,128)(2,1)S(1)}, u32[]{:S(2)}, u32[]{:S(2)}) collective-permute-start(bf16[32,2048]{1,0:T(8,128)(2,1)S(1)} %get-tuple-element.54.refs_0_), channel_id=1, source_target_pairs={{0,24},{8,0},{16,8},{24,16},{1,25},{9,1},{17,9},{25,17},{2,26},{10... | collective-permute-start | bytes 393224 | tf_op jit(solution)/shard_map/ppermute | solution.py:149
  115.7 3.4 %collective-permute-done.18 = bf16[256,256]{1,0:T(8,128)(2,1)S(1)} collective-permute-done((bf16[256,256]{1,0:T(8,128)(2,1)S(1)}, bf16[256,256]{1,0:T(8,128)(2,1)S(1)}, u32[]{:S(2)}, u32[]{:S(2)}) %collective-permute-start.18) | collective-permute-done | bytes 131104 | tf_op jit(solution)/shard_map/ppermute | solution.py:143
  120.9 3.2 %collective-permute-done.16 = bf16[256,256]{1,0:T(8,128)(2,1)S(1)} collective-permute-done((bf16[256,256]{1,0:T(8,128)(2,1)S(1)}, bf16[256,256]{1,0:T(8,128)(2,1)S(1)}, u32[]{:S(2)}, u32[]{:S(2)}) %collective-permute-start.16) | collective-permute-done | bytes 131104 | tf_op jit(solution)/shard_map/ppermute | solution.py:143
  125.8 2.5 %collective-permute-done.19 = bf16[128,256]{1,0:T(8,128)(2,1)S(1)} collective-permute-done((bf16[128,256]{1,0:T(8,128)(2,1)S(1)}, bf16[128,256]{1,0:T(8,128)(2,1)S(1)}, u32[]{:S(2)}, u32[]{:S(2)}) %collective-permute-start.19) | collective-permute-done | bytes 65568 | tf_op jit(solution)/shard_map/ppermute | solution.py:143
  129.8 2.8 %collective-permute-done.17 = bf16[128,256]{1,0:T(8,128)(2,1)S(1)} collective-permute-done((bf16[128,256]{1,0:T(8,128)(2,1)S(1)}, bf16[128,256]{1,0:T(8,128)(2,1)S(1)}, u32[]{:S(2)}, u32[]{:S(2)}) %collective-permute-start.17) | collective-permute-done | bytes 65568 | tf_op jit(solution)/shard_map/ppermute | solution.py:143
  133.2 2.6 %collective-permute-start.21 = (bf16[32,512]{1,0:T(8,128)(2,1)S(1)}, bf16[32,512]{1,0:T(8,128)(2,1)S(1)}, u32[]{:S(2)}, u32[]{:S(2)}) collective-permute-start(bf16[32,512]{1,0:T(8,128)(2,1)S(1)} %get-tuple-element.86), channel_id=1, source_target_pairs={{0,16},{8,24},{16,0},{24,8},{1,17},{9,25},{17,1},{25,9},{2,18},{10... | collective-permute-start | bytes 98312 | tf_op jit(solution)/shard_map/ppermute | solution.py:149
  147.1 3.2 %collective-permute-start.25 = (bf16[32,512]{1,0:T(8,128)(2,1)S(1)}, bf16[32,512]{1,0:T(8,128)(2,1)S(1)}, u32[]{:S(2)}, u32[]{:S(2)}) collective-permute-start(bf16[32,512]{1,0:T(8,128)(2,1)S(1)} %get-tuple-element.39.refs_0_), channel_id=1, source_target_pairs={{0,24},{8,0},{16,8},{24,16},{1,25},{9,1},{17,9},{25,17},{2,26},{10... | collective-permute-start | bytes 98312 | tf_op jit(solution)/shard_map/ppermute | solution.py:149
  150.4 15.2 %collective-permute-done.25.refs_3_ = bf16[32,512]{1,0:T(8,128)(2,1)S(1)} collective-permute-done((bf16[32,512]{1,0:T(8,128)(2,1)S(1)}, bf16[32,512]{1,0:T(8,128)(2,1)S(1)}, u32[]{:S(2)}, u32[]{:S(2)}) %collective-permute-start.25) | collective-permute-done | bytes 32800 | tf_op jit(solution)/shard_map/ppermute | solution.py:149
  173.2 2.4 %collective-permute-start.38 = (f32[16,128]{1,0:T(8,128)S(1)}, f32[16,128]{1,0:T(8,128)S(1)}, u32[]{:S(2)}, u32[]{:S(2)}) collective-permute-start(f32[16,128]{1,0:T(8,128)S(1)} %add.249.refs_0_), channel_id=1, source_target_pairs={{0,6},{2,4},{4,2},{6,0},{1,7},{3,5},{5,3},{7,1},{8,14},{10,12},{12... | collective-permute-start | bytes 24584 | tf_op jit(solution)/shard_map/ppermute | solution.py:143
  180.1 3.3 %collective-permute-done.50.refs_8_ = bf16[128,1024]{1,0:T(8,128)(2,1)S(1)} collective-permute-done((bf16[128,1024]{1,0:T(8,128)(2,1)S(1)}, bf16[128,1024]{1,0:T(8,128)(2,1)S(1)}, u32[]{:S(2)}, u32[]{:S(2)}) %collective-permute-start.50) | collective-permute-done | bytes 262176 | tf_op jit(solution)/shard_map/ppermute | solution.py:143
  183.4 4.0 %shard_map.184 = (f32[128,2048]{1,0:T(8,128)}, bf16[512,2048]{1,0:T(8,128)(2,1)}) custom-call(s32[1]{0:T(128)} %bitcast.place_ref, f32[16,128]{1,0:T(8,128)S(1)} %add.249.refs_0_, f32[16,128]{1,0:T(8,128)S(1)} %collective-permute-done.36.refs_1_, f32[16,128]{1,0:T(8,128)S(1)} %collective-permute-done.37.refs_2_, ...), custom_call_target="tpu_custom_call" | custom-call | tf_op jit(solution)/shard_map/pallas_call | solution.py:116
  187.5 2.6 %shard_map.183 = (f32[256,512]{1,0:T(8,128)}, bf16[1024,512]{1,0:T(8,128)(2,1)}) custom-call(s32[1]{0:T(128)} %bitcast.place_ref, f32[16,128]{1,0:T(8,128)S(1)} %add.249.refs_0_, f32[16,128]{1,0:T(8,128)S(1)} %collective-permute-done.36.refs_1_, f32[16,128]{1,0:T(8,128)S(1)} %collective-permute-done.37.refs_2_, ...), custom_call_target="tpu_custom_call" | custom-call | tf_op jit(solution)/shard_map/pallas_call | solution.py:116
  (161 shorter events, 80.2 us)
Async XLA Ops:
  11.9 9.5 %collective-permute-start.10 = (bf16[512,256]{1,0:T(8,128)(2,1)S(1)}, bf16[512,256]{1,0:T(8,128)(2,1)S(1)}, u32[]{:S(2)}, u32[]{:S(2)}) collective-permute-start(bf16[512,256]{1,0:T(8,128)(2,1)S(1)} %shard_map.180), channel_id=1, source_target_pairs={{0,6},{2,4},{4,2},{6,0},{1,7},{3,5},{5,3},{7,1},{8,14},{10,12},{12... | collective-permute-start | bytes 786440 | tf_op jit(solution)/shard_map/ppermute | solution.py:143
  14.4 11.9 %collective-permute-start.9 = (bf16[512,256]{1,0:T(8,128)(2,1)S(1)}, bf16[512,256]{1,0:T(8,128)(2,1)S(1)}, u32[]{:S(2)}, u32[]{:S(2)}) collective-permute-start(bf16[512,256]{1,0:T(8,128)(2,1)S(1)} %shard_map.180), channel_id=1, source_target_pairs={{0,4},{2,6},{4,0},{6,2},{1,5},{3,7},{5,1},{7,3},{8,12},{10,14},{12... | collective-permute-start | bytes 786440 | tf_op jit(solution)/shard_map/ppermute | solution.py:143
  15.0 14.6 %collective-permute-start = (bf16[256,256]{1,0:T(8,128)(2,1)S(1)}, bf16[256,256]{1,0:T(8,128)(2,1)S(1)}, u32[]{:S(2)}, u32[]{:S(2)}) collective-permute-start(bf16[256,256]{1,0:T(8,128)(2,1)S(1)} %constant_dynamic-slice_fusion.15.refs_0_), channel_id=1, source_target_pairs={{0,8},{8,16},{16,24},{24,0},{1,9},{9,17},{17,25},{25,1},{2,10},{10... | collective-permute-start | bytes 393224 | tf_op jit(solution)/shard_map/ppermute | solution.py:149
  16.6 12.9 %collective-permute-start.1 = (bf16[256,256]{1,0:T(8,128)(2,1)S(1)}, bf16[256,256]{1,0:T(8,128)(2,1)S(1)}, u32[]{:S(2)}, u32[]{:S(2)}) collective-permute-start(bf16[256,256]{1,0:T(8,128)(2,1)S(1)} %constant_dynamic-slice_fusion.15.refs_0_), channel_id=1, source_target_pairs={{0,16},{8,24},{16,0},{24,8},{1,17},{9,25},{17,1},{25,9},{2,18},{10... | collective-permute-start | bytes 393224 | tf_op jit(solution)/shard_map/ppermute | solution.py:149
  18.6 11.0 %collective-permute-start.2 = (bf16[256,256]{1,0:T(8,128)(2,1)S(1)}, bf16[256,256]{1,0:T(8,128)(2,1)S(1)}, u32[]{:S(2)}, u32[]{:S(2)}) collective-permute-start(bf16[256,256]{1,0:T(8,128)(2,1)S(1)} %constant_dynamic-slice_fusion.15.refs_0_), channel_id=1, source_target_pairs={{0,24},{8,0},{16,8},{24,16},{1,25},{9,1},{17,9},{25,17},{2,26},{10... | collective-permute-start | bytes 393224 | tf_op jit(solution)/shard_map/ppermute | solution.py:149
  29.6 14.4 %collective-permute-start.3 = (bf16[1024,256]{1,0:T(8,128)(2,1)S(1)}, bf16[1024,256]{1,0:T(8,128)(2,1)S(1)}, u32[]{:S(2)}, u32[]{:S(2)}) collective-permute-start(bf16[1024,256]{1,0:T(8,128)(2,1)S(1)} %shard_map.179), channel_id=1, source_target_pairs={{0,2},{2,0},{4,6},{6,4},{1,3},{3,1},{5,7},{7,5},{8,10},{10,8},{12,... | collective-permute-start | bytes 1572872 | tf_op jit(solution)/shard_map/ppermute | solution.py:143
  30.5 14.8 %collective-permute-start.4 = (bf16[1024,256]{1,0:T(8,128)(2,1)S(1)}, bf16[1024,256]{1,0:T(8,128)(2,1)S(1)}, u32[]{:S(2)}, u32[]{:S(2)}) collective-permute-start(bf16[1024,256]{1,0:T(8,128)(2,1)S(1)} %shard_map.179), channel_id=1, source_target_pairs={{0,4},{2,6},{4,0},{6,2},{1,5},{3,7},{5,1},{7,3},{8,12},{10,14},{12... | collective-permute-start | bytes 1572872 | tf_op jit(solution)/shard_map/ppermute | solution.py:143
  31.8 49.1 %collective-permute-start.44 = (bf16[128,3072]{1,0:T(8,128)(2,1)S(1)}, bf16[128,3072]{1,0:T(8,128)(2,1)S(1)}, u32[]{:S(2)}, u32[]{:S(2)}) collective-permute-start(bf16[128,3072]{1,0:T(8,128)(2,1)S(1)} %pad_maximum_fusion.1.refs_10_.refs_11_), channel_id=1, source_target_pairs={{0,8},{8,16},{16,24},{24,0},{1,9},{9,17},{17,25},{25,1},{2,10},{10... | collective-permute-start | bytes 2359304 | tf_op jit(solution)/shard_map/ppermute | solution.py:149
  35.9 20.6 %collective-permute-start.14 = (bf16[256,1024]{1,0:T(8,128)(2,1)S(1)}, bf16[256,1024]{1,0:T(8,128)(2,1)S(1)}, u32[]{:S(2)}, u32[]{:S(2)}) collective-permute-start(bf16[256,1024]{1,0:T(8,128)(2,1)S(1)} %fusion.36), channel_id=1, source_target_pairs={{0,4},{2,6},{4,0},{6,2},{1,5},{3,7},{5,1},{7,3},{8,12},{10,14},{12... | collective-permute-start | bytes 1572872 | tf_op jit(solution)/shard_map/ppermute | solution.py:143
  45.3 13.1 %collective-permute-start.12 = (bf16[512,256]{1,0:T(8,128)(2,1)S(1)}, bf16[512,256]{1,0:T(8,128)(2,1)S(1)}, u32[]{:S(2)}, u32[]{:S(2)}) collective-permute-start(bf16[512,256]{1,0:T(8,128)(2,1)S(1)} %slice.63), channel_id=1, source_target_pairs={{0,2},{2,0},{4,6},{6,4},{1,3},{3,1},{5,7},{7,5},{8,10},{10,8},{12,... | collective-permute-start | bytes 786440 | tf_op jit(solution)/shard_map/ppermute | solution.py:143
  46.6 14.7 %collective-permute-start.13 = (bf16[512,256]{1,0:T(8,128)(2,1)S(1)}, bf16[512,256]{1,0:T(8,128)(2,1)S(1)}, u32[]{:S(2)}, u32[]{:S(2)}) collective-permute-start(bf16[512,256]{1,0:T(8,128)(2,1)S(1)} %slice.64), channel_id=1, source_target_pairs={{0,4},{2,6},{4,0},{6,2},{1,5},{3,7},{5,1},{7,3},{8,12},{10,14},{12... | collective-permute-start | bytes 786440 | tf_op jit(solution)/shard_map/ppermute | solution.py:143
  48.9 16.8 %collective-permute-start.26 = (bf16[256,1024]{1,0:T(8,128)(2,1)S(1)}, bf16[256,1024]{1,0:T(8,128)(2,1)S(1)}, u32[]{:S(2)}, u32[]{:S(2)}) collective-permute-start(bf16[256,1024]{1,0:T(8,128)(2,1)S(1)} %fusion.39), channel_id=1, source_target_pairs={{0,2},{2,0},{4,6},{6,4},{1,3},{3,1},{5,7},{7,5},{8,10},{10,8},{12,... | collective-permute-start | bytes 1572872 | tf_op jit(solution)/shard_map/ppermute | solution.py:143
  57.1 11.9 %collective-permute-start.28 = (bf16[128,1024]{1,0:T(8,128)(2,1)S(1)}, bf16[128,1024]{1,0:T(8,128)(2,1)S(1)}, u32[]{:S(2)}, u32[]{:S(2)}) collective-permute-start(bf16[128,1024]{1,0:T(8,128)(2,1)S(1)} %fusion.63), channel_id=1, source_target_pairs={{0,2},{2,0},{4,6},{6,4},{1,3},{3,1},{5,7},{7,5},{8,10},{10,8},{12,... | collective-permute-start | bytes 786440 | tf_op jit(solution)/shard_map/ppermute | solution.py:143
  80.8 31.6 %collective-permute-start.15 = (bf16[1024,256]{1,0:T(8,128)(2,1)}, bf16[1024,256]{1,0:T(8,128)(2,1)}, u32[]{:S(2)}, u32[]{:S(2)}) collective-permute-start(bf16[1024,256]{1,0:T(8,128)(2,1)} %fusion.32), channel_id=1, source_target_pairs={{0,1},{1,0},{2,3},{3,2},{4,5},{5,4},{6,7},{7,6},{8,9},{9,8},{10,11... | collective-permute-start | bytes 1572872 | tf_op jit(solution)/shard_map/ppermute | solution.py:146
  80.8 63.5 %collective-permute-start.45 = (bf16[128,3072]{1,0:T(8,128)(2,1)S(1)}, bf16[128,3072]{1,0:T(8,128)(2,1)S(1)}, u32[]{:S(2)}, u32[]{:S(2)}) collective-permute-start(bf16[128,3072]{1,0:T(8,128)(2,1)S(1)} %collective-permute-done.44.refs_12_.refs_13_.refs_11_), channel_id=1, source_target_pairs={{0,8},{8,16},{16,24},{24,0},{1,9},{9,17},{17,25},{25,1},{2,10},{10... | collective-permute-start | bytes 2359304 | tf_op jit(solution)/shard_map/ppermute | solution.py:149
  86.8 46.4 %collective-permute-start.32 = (bf16[32,2048]{1,0:T(8,128)(2,1)S(1)}, bf16[32,2048]{1,0:T(8,128)(2,1)S(1)}, u32[]{:S(2)}, u32[]{:S(2)}) collective-permute-start(bf16[32,2048]{1,0:T(8,128)(2,1)S(1)} %get-tuple-element.54.refs_0_), channel_id=1, source_target_pairs={{0,8},{8,16},{16,24},{24,0},{1,9},{9,17},{17,25},{25,1},{2,10},{10... | collective-permute-start | bytes 393224 | tf_op jit(solution)/shard_map/ppermute | solution.py:149
  110.0 25.7 %collective-permute-start.33 = (bf16[32,2048]{1,0:T(8,128)(2,1)S(1)}, bf16[32,2048]{1,0:T(8,128)(2,1)S(1)}, u32[]{:S(2)}, u32[]{:S(2)}) collective-permute-start(bf16[32,2048]{1,0:T(8,128)(2,1)S(1)} %get-tuple-element.54.refs_0_), channel_id=1, source_target_pairs={{0,16},{8,24},{16,0},{24,8},{1,17},{9,25},{17,1},{25,9},{2,18},{10... | collective-permute-start | bytes 393224 | tf_op jit(solution)/shard_map/ppermute | solution.py:149
  110.0 27.0 %collective-permute-start.34 = (bf16[32,2048]{1,0:T(8,128)(2,1)S(1)}, bf16[32,2048]{1,0:T(8,128)(2,1)S(1)}, u32[]{:S(2)}, u32[]{:S(2)}) collective-permute-start(bf16[32,2048]{1,0:T(8,128)(2,1)S(1)} %get-tuple-element.54.refs_0_), channel_id=1, source_target_pairs={{0,24},{8,0},{16,8},{24,16},{1,25},{9,1},{17,9},{25,17},{2,26},{10... | collective-permute-start | bytes 393224 | tf_op jit(solution)/shard_map/ppermute | solution.py:149
  138.9 28.9 %collective-permute-start.39 = (bf16[1024,256]{1,0:T(8,128)(2,1)S(1)}, bf16[1024,256]{1,0:T(8,128)(2,1)S(1)}, u32[]{:S(2)}, u32[]{:S(2)}) collective-permute-start(bf16[1024,256]{1,0:T(8,128)(2,1)S(1)} %shard_map.179), channel_id=1, source_target_pairs={{0,1},{1,0},{2,3},{3,2},{4,5},{5,4},{6,7},{7,6},{8,9},{9,8},{10,11... | collective-permute-start | bytes 1572872 | tf_op jit(solution)/shard_map/ppermute | solution.py:146
  138.9 30.0 %collective-permute-start.49 = (bf16[128,2048]{1,0:T(8,128)(2,1)S(1)}, bf16[128,2048]{1,0:T(8,128)(2,1)S(1)}, u32[]{:S(2)}, u32[]{:S(2)}) collective-permute-start(bf16[128,2048]{1,0:T(8,128)(2,1)S(1)} %get-tuple-element.38.refs_5_), channel_id=1, source_target_pairs={{0,4},{2,6},{4,0},{6,2},{1,5},{3,7},{5,1},{7,3},{8,12},{10,14},{12... | collective-permute-start | bytes 1572872 | tf_op jit(solution)/shard_map/ppermute | solution.py:143
  144.4 25.5 %collective-permute-start.48 = (bf16[128,2048]{1,0:T(8,128)(2,1)S(1)}, bf16[128,2048]{1,0:T(8,128)(2,1)S(1)}, u32[]{:S(2)}, u32[]{:S(2)}) collective-permute-start(bf16[128,2048]{1,0:T(8,128)(2,1)S(1)} %get-tuple-element.38.refs_5_), channel_id=1, source_target_pairs={{0,2},{2,0},{4,6},{6,4},{1,3},{3,1},{5,7},{7,5},{8,10},{10,8},{12,... | collective-permute-start | bytes 1572872 | tf_op jit(solution)/shard_map/ppermute | solution.py:143
  146.5 33.6 %collective-permute-start.46 = (bf16[128,3072]{1,0:T(8,128)(2,1)S(1)}, bf16[128,3072]{1,0:T(8,128)(2,1)S(1)}, u32[]{:S(2)}, u32[]{:S(2)}) collective-permute-start(bf16[128,3072]{1,0:T(8,128)(2,1)S(1)} %collective-permute-done.45.refs_14_.refs_15_.refs_12_), channel_id=1, source_target_pairs={{0,8},{8,16},{16,24},{24,0},{1,9},{9,17},{17,25},{25,1},{2,10},{10... | collective-permute-start | bytes 2359304 | tf_op jit(solution)/shard_map/ppermute | solution.py:149
  147.1 18.5 %collective-permute-start.25 = (bf16[32,512]{1,0:T(8,128)(2,1)S(1)}, bf16[32,512]{1,0:T(8,128)(2,1)S(1)}, u32[]{:S(2)}, u32[]{:S(2)}) collective-permute-start(bf16[32,512]{1,0:T(8,128)(2,1)S(1)} %get-tuple-element.39.refs_0_), channel_id=1, source_target_pairs={{0,24},{8,0},{16,8},{24,16},{1,25},{9,1},{17,9},{25,17},{2,26},{10... | collective-permute-start | bytes 98312 | tf_op jit(solution)/shard_map/ppermute | solution.py:149
  176.9 10.5 %collective-permute-start.42 = (bf16[128,256]{1,0:T(8,128)(2,1)S(1)}, bf16[128,256]{1,0:T(8,128)(2,1)S(1)}, u32[]{:S(2)}, u32[]{:S(2)}) collective-permute-start(bf16[128,256]{1,0:T(8,128)(2,1)S(1)} %slice.90), channel_id=1, source_target_pairs={{0,2},{2,0},{4,6},{6,4},{1,3},{3,1},{5,7},{7,5},{8,10},{10,8},{12,... | collective-permute-start | bytes 196616 | tf_op jit(solution)/shard_map/ppermute | solution.py:143
  (38 other events, 311.5 us)
